TPU v7x, 128 devices: a whole 4x4x4 slice. The times are simulated.
128 devices in a mesh: rep: 2 (over z_hi), fs: 32 (over z_lo, y, x), tp: 2 (over core).
Axes of the slice: x: 4, y: 4, z: 4 (z_hi: 2, z_lo: 2; z = z_hi * 2 + z_lo), core: 2. Of those that a mesh axis runs over, the one named last changes fastest.
Arguments:
- tokens: bfloat16 [49152, 2048], P(('rep', 'fs', 'tp')), may hold values from -6 to 6
- outer_weight: float32 [2048, 1536], P('fs', 'tp'), may hold values from -0.125 to 0.125
- inner_weight: float32 [2048, 1536], P('fs', 'tp'), may hold values from -0.125 to 0.125
- value_weight: float32 [2048, 1536], P('fs', 'tp'), may hold values from -0.125 to 0.125
- conv_taps: float32 [3, 1536], P(None, 'tp'), may hold values from -3 to 3
- mix_out: float32 [1536, 2048], P('tp', 'fs'), may hold values from -0.15625 to 0.15625
- norm_first: float32 [2048], replicated, may hold values from 0.1 to 1.9
- up_weight: float32 [2048, 4096], P('fs', 'tp'), may hold values from -0.125 to 0.125
- down_weight: float32 [4096, 2048], P('tp', 'fs'), may hold values from -0.09375 to 0.09375
- norm_second: float32 [2048], replicated, may hold values from 0.1 to 1.9
Outputs:
- encoded: bfloat16 [49152, 2048], P(('rep', 'fs', 'tp'))
All inputs are finite; a program needn't handle non-finite values.
Results may differ from a plain program's by a relative error of at most 0.015.
Values may be sent and summed in bfloat16 or wider, within the bound.
No kernel may reach another device: no remote copies, remote signals or barrier semaphores. Data moves between devices by JAX's collectives and lax.ppermute only.
A program may use at most 128 MiB of HBM per device.

v0:
```python
import jax
import jax.numpy as jnp
from jax import lax
from jax.sharding import Mesh
from jax.sharding import PartitionSpec as P

SEQ = 128
FS = ("fs_0", "fs_1", "fs_2")
REP_FS_TP = ("rep", "fs_0", "fs_1", "fs_2", "tp")
residual_scale = 2.0**0.25
norm_epsilon = 1e-05


def in_one_piece(arrays, axis, dim, along):
    ends, at = ([], 0)
    for a in arrays[:-1]:
        at += a.shape[along]
        ends.append(at)
    both = jnp.concatenate(arrays, axis=along)
    return tuple(jnp.split(lax.all_gather(both, axis, axis=dim, tiled=True), ends, axis=along))


def laid_out(tiles, dim):
    tiles = jnp.moveaxis(tiles, 0, dim)
    lengths = tiles.shape
    return tiles.reshape(*lengths[:dim], lengths[dim] * lengths[dim + 1], *lengths[dim + 2 :])


def stacked_from(x, axes, order):
    tiles = x
    for k in order:
        tiles = lax.all_gather(tiles, axes[k])
    done = order[::-1]
    back = [done.index(k) for k in range(len(axes))]
    tiles = tiles.transpose(*back, *range(len(axes), tiles.ndim))
    return tiles.reshape(-1, *x.shape)


def whole_of(x, axes, order, dim):
    return laid_out(stacked_from(x, axes, order), dim)


def cut_along(x, dim, length):
    before, after = (x.shape[:dim], x.shape[dim + 1 :])
    return jnp.moveaxis(x.reshape(*before, length, -1, *after), dim, 0)


def sum_at_owner(x, axis, dim):
    tiles = cut_along(x, dim, lax.axis_size(axis))
    arrived = lax.all_to_all(tiles, axis, split_axis=0, concat_axis=0, tiled=True)
    return arrived.astype(jnp.float32).sum(axis=0)


def layer_norm(values, scaling):
    center = values - jnp.mean(values, axis=-1, keepdims=True)
    spread = jnp.mean(center * center, axis=-1, keepdims=True)
    return center * lax.rsqrt(spread + norm_epsilon) * scaling


def short_conv(product, conv_taps):
    places = jnp.arange(product.shape[0], dtype=jnp.int32) % SEQ
    blank = jnp.zeros((1, product.shape[1]), jnp.float32)
    before = jnp.concatenate([blank, product[:-1]], axis=0)
    after = jnp.concatenate([product[1:], blank], axis=0)
    before = jnp.where((places > 0)[:, None], before, 0.0)
    after = jnp.where((places < SEQ - 1)[:, None], after, 0.0)
    return conv_taps[0] * before + conv_taps[1] * product + conv_taps[2] * after


def local(
    tokens,
    outer_weight,
    inner_weight,
    value_weight,
    conv_taps,
    mix_out,
    norm_first,
    up_weight,
    down_weight,
    norm_second,
):
    grouped = lax.all_gather(tokens, "tp", axis=0, tiled=True)
    outer_bf = outer_weight.astype(jnp.bfloat16)
    inner_bf = inner_weight.astype(jnp.bfloat16)
    value_bf = value_weight.astype(jnp.bfloat16)
    outer_full, inner_full, value_full = in_one_piece((outer_bf, inner_bf, value_bf), FS, 0, 1)
    outer = jnp.dot(grouped, outer_full, preferred_element_type=jnp.float32)
    inner = jnp.dot(grouped, inner_full, preferred_element_type=jnp.float32)
    value = jnp.dot(grouped, value_full, preferred_element_type=jnp.float32)
    mixed = (outer * short_conv(inner * value, conv_taps)).astype(jnp.bfloat16)
    mixout_full = whole_of(mix_out.astype(jnp.bfloat16), FS, (0, 1, 2), 1)
    selected = mixed
    mixing = sum_at_owner(
        jnp.dot(selected, mixout_full, preferred_element_type=jnp.float32).astype(jnp.bfloat16),
        "tp",
        0,
    )
    first = layer_norm(residual_scale * tokens.astype(jnp.float32) + mixing, norm_first).astype(
        jnp.bfloat16
    )
    grouped_first = lax.all_gather(first, "tp", axis=0, tiled=True)
    upward_bf = up_weight.astype(jnp.bfloat16)
    upward_full = lax.all_gather(upward_bf, FS, axis=0, tiled=True)
    raised = jnp.dot(grouped_first, upward_full, preferred_element_type=jnp.float32)
    raised = jax.nn.relu(raised)
    hidden = (raised * raised).astype(jnp.bfloat16)
    down_full = lax.all_gather(down_weight.astype(jnp.bfloat16), FS, axis=1, tiled=True)
    selected = hidden
    lowered = sum_at_owner(
        jnp.dot(selected, down_full, preferred_element_type=jnp.float32).astype(jnp.bfloat16),
        "tp",
        0,
    )
    return layer_norm(residual_scale * first.astype(jnp.float32) + lowered, norm_second).astype(
        jnp.bfloat16
    )


def solution(mesh):
    finer = Mesh(
        mesh.devices.reshape(mesh.shape["rep"], 2, 4, 4, mesh.shape["tp"]),
        ("rep", "fs_0", "fs_1", "fs_2", "tp"),
    )
    placed = (
        P(REP_FS_TP, None),
        P(FS, "tp"),
        P(FS, "tp"),
        P(FS, "tp"),
        P(None, "tp"),
        P("tp", FS),
        P(),
        P(FS, "tp"),
        P("tp", FS),
        P(),
    )
    return jax.shard_map(
        local, mesh=finer, in_specs=placed, out_specs=P(REP_FS_TP, None), check_vma=False
    )
```

profile of v0, /device:TPU:1, one launch (start us, length us, event | category | flops | bytes accessed | tf_op | source)
XLA Modules:
  0.0 637.7 jit_solution(7984287710747323062)
XLA Ops:
  6.5 0.0 all-gather.20.cloned.1.call-start
  6.6 1.0 convert_element_type.53
  7.6 5.6 all-gather
  13.2 0.0 copy-start.9
  13.3 13.2 %all-gather.1 = bf16[8,768,64]{1,2,0:T(8,128)(2,1)} all-gather(bf16[2,768,64]{1,2,0:T(8,128)(2,1)S(1)} %bitcast.37), channel_id=3, replica_groups=mesh['rep'=2,'fs_0'=2,'fs_1'=4,'fs_2'=4,'tp'=2] {'fs_1'}, dimensions={0}, use_global_device_ids=true | all-gather | bytes 983040 | tf_op jit(solution)/shard_map/all_gather | solution.py:32
  26.5 0.0 all-gather.20.cloned.1.call-update
  26.5 0.0 all-gather.12.cloned.1.call-start
  26.6 0.7 all-gather.12.cloned.1.call-update
  27.3 0.0 all-gather.10.cloned.1.call-start
  27.3 0.0 copy-done.4
  27.3 0.0 copy-done.5
  27.4 0.7 pad_maximum_fusion
  28.1 0.0 all-gather.10.cloned.1.call-update
  28.2 0.0 all-gather.16.cloned.1.call-start
  28.2 0.7 convert_element_type.58
  29.0 0.0 all-gather.16.cloned.1.call-update
  29.0 0.0 all-gather.14.cloned.1.call-start
  29.0 0.0 copy-done.9
  29.1 41.1 %all-gather.20.cloned.1.call-done = bf16[16,2,768,64]{2,3,1,0:T(8,128)(2,1)} async-done(((bf16[4,2,768,64]{2,3,1,0:T(8,128)(2,1)}), bf16[16,2,768,64]{2,3,1,0:T(8,128)(2,1)}) %all-gather.20.cloned.1.call-update) | async-done | bytes 3145744 | tf_op jit(solution)/shard_map/all_gather | solution.py:32
  70.2 3.9 copy.15
  74.1 13.4 %all-gather.12.cloned.1.call-done = bf16[768,2048]{1,0:T(8,128)(2,1)} async-done(((bf16[384,2048]{1,0:T(8,128)(2,1)}), bf16[768,2048]{1,0:T(8,128)(2,1)}) %all-gather.12.cloned.1.call-update) | async-done | bytes 3145744 | tf_op jit(solution)/shard_map/all_gather | solution.py:82
  87.5 149.6 %all-gather.10.cloned.1.call-done = bf16[2048,2304]{1,0:T(8,128)(2,1)} async-done(((bf16[64,2304]{1,0:T(8,128)(2,1)}), bf16[2048,2304]{1,0:T(8,128)(2,1)}) %all-gather.10.cloned.1.call-update) | async-done | bytes 9437200 | tf_op jit(solution)/shard_map/all_gather | solution.py:20
  237.1 5.6 fusion
  242.8 4.6 multiply_bitcast_fusion
  247.3 2.9 fusion.21
  250.3 13.9 %convolution_convert_fusion.1 = bf16[768,2048]{1,0:T(8,128)(2,1)} fusion(bf16[768,2048]{0,1:T(8,128)(2,1)} %bitcast.32, f32[767,768]{0,1:T(8,128)} %get-tuple-element.9, f32[768,768]{0,1:T(8,128)S(1)} %multiply_bitcast_fusion, f32[767,768]{0,1:T(8,128)} %get-tuple-element.8, bf16[768,2048]{1,0:T(8,128)(2,1)} %all-gather.12.cloned.1.call-done, ...), kind=kOutput, calls=%fused_computation.4 | convolution fusion | flops 4838719488 | bytes 19671552 | tf_op jit(solution)/shard_map/dot_general | solution.py:94
  264.2 28.7 %all_to_all.10 = bf16[2,384,2048]{2,1,0:T(8,128)(2,1)S(1)} all-to-all(bf16[2,384,2048]{2,1,0:T(8,128)(2,1)} %bitcast.33), channel_id=1, replica_groups=mesh['rep'=2,'fs_0'=2,'fs_1'=4,'fs_2'=4,'tp'=2] {'tp'}, dimensions={0} | all-to-all | bytes 6291456 | tf_op jit(solution)/shard_map/all_to_all | solution.py:50
  292.8 0.7 convert_reduce_fusion.1
  293.6 0.7 copy-done.1
  294.2 0.5 fusion.11
  294.7 0.7 multiply_reduce_fusion.1
  295.5 0.0 copy-start.3
  295.5 1.8 multiply_convert_fusion.2
  297.3 0.0 all-gather.14.cloned.1.call-update
  297.3 0.0 all-gather.18.cloned.1.call-start
  297.4 0.8 convert_element_type.60
  298.2 0.0 all-gather.18.cloned.1.call-update
  298.2 106.1 %all-gather.16.cloned.1.call-done = bf16[2048,2048]{1,0:T(8,128)(2,1)} async-done(((bf16[64,2048]{1,0:T(8,128)(2,1)}), bf16[2048,2048]{1,0:T(8,128)(2,1)}) %all-gather.16.cloned.1.call-update) | async-done | bytes 8388624 | tf_op jit(solution)/shard_map/all_gather | solution.py:103
  404.2 37.8 %all-gather.14.cloned.1.call-done = bf16[768,2048]{1,0:T(8,128)(2,1)} async-done(((bf16[384,2048]{1,0:T(8,128)(2,1)}), bf16[768,2048]{1,0:T(8,128)(2,1)}) %all-gather.14.cloned.1.call-update) | async-done | bytes 3145744 | tf_op jit(solution)/shard_map/all_gather | solution.py:101
  442.1 10.0 %multiply_convert_fusion = bf16[768,2048]{1,0:T(8,128)(2,1)S(1)} fusion(bf16[768,2048]{1,0:T(8,128)(2,1)} %all-gather.14.cloned.1.call-done, bf16[2048,2048]{1,0:T(8,128)(2,1)} %all-gather.16.cloned.1.call-done), kind=kOutput, calls=%fused_computation.1 | convolution fusion | flops 6447169536 | bytes 14680064 | tf_op jit(solution)/shard_map/dot_general | solution.py:104
  452.1 138.3 %all-gather.18.cloned.1.call-done = bf16[2048,2048]{0,1:T(8,128)(2,1)} async-done(((bf16[2048,64]{0,1:T(8,128)(2,1)}), bf16[2048,2048]{0,1:T(8,128)(2,1)}) %all-gather.18.cloned.1.call-update) | async-done | bytes 8388624 | tf_op jit(solution)/shard_map/all_gather | solution.py:107
  590.4 9.1 %convolution_convert_fusion = bf16[768,2048]{1,0:T(8,128)(2,1)S(1)} fusion(bf16[768,2048]{1,0:T(8,128)(2,1)S(1)} %multiply_convert_fusion, bf16[2048,2048]{0,1:T(8,128)(2,1)} %all-gather.18.cloned.1.call-done), kind=kOutput, calls=%fused_computation.3 | convolution fusion | flops 6444023808 | bytes 14680064 | tf_op jit(solution)/shard_map/dot_general | solution.py:110
  599.5 26.9 %all_to_all.11 = bf16[2,384,2048]{2,1,0:T(8,128)(2,1)S(1)} all-to-all(bf16[2,384,2048]{2,1,0:T(8,128)(2,1)S(1)} %bitcast.34), channel_id=1, replica_groups=mesh['rep'=2,'fs_0'=2,'fs_1'=4,'fs_2'=4,'tp'=2] {'tp'}, dimensions={0} | all-to-all | bytes 6291456 | tf_op jit(solution)/shard_map/all_to_all | solution.py:50
  626.4 0.7 convert_reduce_fusion
  627.2 0.7 copy-done
  627.8 0.5 fusion.12
  628.3 0.7 multiply_reduce_fusion
  629.1 1.8 multiply_convert_fusion.1
  (25 shorter events, 0.1 us)
Async XLA Ops:
  6.5 20.8 %copy-start.4 = (f32[64,768]{1,0:T(8,128)S(1)}, f32[64,768]{1,0:T(8,128)}, u32[]{:S(2)}) copy-start(f32[64,768]{1,0:T(8,128)} %param.11) | copy-start | bytes 589828
  6.5 20.8 %copy-start.5 = (f32[64,768]{1,0:T(8,128)S(1)}, f32[64,768]{1,0:T(8,128)}, u32[]{:S(2)}) copy-start(f32[64,768]{1,0:T(8,128)} %param.12) | copy-start | bytes 589828
  6.5 20.8 %copy-start.6 = (f32[64,768]{1,0:T(8,128)S(1)}, f32[64,768]{1,0:T(8,128)}, u32[]{:S(2)}) copy-start(f32[64,768]{1,0:T(8,128)} %param.13) | copy-start | bytes 589828
  6.5 21.7 %copy-start.2 = (f32[64,2048]{1,0:T(8,128)S(1)}, f32[64,2048]{1,0:T(8,128)}, u32[]{:S(2)}) copy-start(f32[64,2048]{1,0:T(8,128)} %param.17) | copy-start | bytes 1572868
  6.5 63.7 %all-gather.20.cloned.1.call-start = ((), (), s32[]{:S(2)}) async-start(), calls=%async_computation.7 | async-start | bytes 3932160 | tf_op jit(solution)/shard_map/all_gather | solution.py:32
  13.2 15.8 %copy-start.9 = (f32[3,768]{1,0:T(4,128)S(1)}, f32[3,768]{1,0:T(4,128)}, u32[]{:S(2)}) copy-start(f32[3,768]{1,0:T(4,128)} %param.14) | copy-start | bytes 27652
  26.5 61.0 %all-gather.12.cloned.1.call-start = ((), (), s32[]{:S(2)}) async-start(), calls=%async_computation.3 | async-start | bytes 4718592 | tf_op jit(solution)/shard_map/all_gather | solution.py:82
  27.3 209.8 %all-gather.10.cloned.1.call-start = ((), (), s32[]{:S(2)}) async-start(), calls=%async_computation.2 | async-start | bytes 9732096 | tf_op jit(solution)/shard_map/all_gather | solution.py:20
  28.2 376.1 %all-gather.16.cloned.1.call-start = ((), (), s32[]{:S(2)}) async-start(), calls=%async_computation.5 | async-start | bytes 8650752 | tf_op jit(solution)/shard_map/all_gather | solution.py:103
  29.0 413.1 %all-gather.14.cloned.1.call-start = ((), (), s32[]{:S(2)}) async-start(), calls=%async_computation.4 | async-start | bytes 4718592 | tf_op jit(solution)/shard_map/all_gather | solution.py:101
  237.1 5.7 copy-start.10
  292.8 1.4 copy-start.1
  294.7 0.7 copy-start.7
  295.5 1.9 copy-start.3
  297.3 293.0 %all-gather.18.cloned.1.call-start = ((), (), s32[]{:S(2)}) async-start(), calls=%async_computation.6 | async-start | bytes 8650752 | tf_op jit(solution)/shard_map/all_gather | solution.py:107
  626.4 1.4 copy-start
  628.3 0.7 copy-start.8
Sparse Core Ops, SparseCore 0:
  26.6 43.5 all-gather.19
  71.9 15.6 all-gather.11
  89.2 147.8 all-gather.9
  238.6 165.6 all-gather.15
  405.7 36.2 all-gather.13
  443.6 146.7 all-gather.17
where the time goes:
time: 638 us
  waiting for transfers between devices  487 us (76%)
  blocking collectives  74.4 us (12%)
  matrix products  43.3 us (7%)
  between operations  13.7 us (2%)
  other arithmetic  10.8 us (2%)
  local copies, waits for them, and re-layouts  8.27 us (1%)
    all_gather x1, waiting for transfers between devices, in_one_piece(): lax.all_gather(both, axis, axis=dim, tiled=True)  150 us
    all_gather x1, waiting for transfers between devices, local(): lax.all_gather(down_weight.astype(jnp.bfloat16), FS, axis=1, tiled=True)  138 us
    all_gather x1, waiting for transfers between devices, local(): upward_full = lax.all_gather(upward_bf, FS, axis=0, tiled=True)  106 us
    all_to_all x2, blocking collectives, sum_at_owner(): lax.all_to_all(tiles, axis, split_axis=0, concat_axis=0, tiled=True)  55.6 us
    all_gather x1, waiting for transfers between devices, stacked_from(): tiles = lax.all_gather(tiles, axes[k])  41.1 us
    all_gather x1, waiting for transfers between devices, local(): grouped_first = lax.all_gather(first, 'tp', axis=0, tiled=True)  37.8 us
    all_gather x2, blocking collectives, stacked_from(): tiles = lax.all_gather(tiles, axes[k])  18.8 us
    dot_general x1, matrix products, local(): jnp.dot(selected, mixout_full, preferred_element_type=jnp.float32)  13.9 us
  transfers between devices with their start and end apart: 6, of which 6 were waited for; matrix products, arithmetic and copies ran while one was open for 7% of the time, Pallas kernels for 0%

commit v1 on v0

--- a/solution.py
+++ b/solution.py
@@ -104,7 +104,10 @@
     raised = jnp.dot(grouped_first, upward_full, preferred_element_type=jnp.float32)
     raised = jax.nn.relu(raised)
     hidden = (raised * raised).astype(jnp.bfloat16)
-    down_full = lax.all_gather(down_weight.astype(jnp.bfloat16), FS, axis=1, tiled=True)
+    down_full = jnp.concatenate(
+        lax.all_to_all(jnp.stack([down_weight.astype(jnp.bfloat16)] * lax.axis_size(FS)), FS, 0, 0),
+        axis=1,
+    )
     selected = hidden
     lowered = sum_at_owner(
         jnp.dot(selected, down_full, preferred_element_type=jnp.float32).astype(jnp.bfloat16),

time: 638 us -> 559 us (0.88)
  waiting for transfers between devices: 487 us -> 414 us
  blocking collectives: 74.4 us -> 56.6 us
  starting transfers between devices: 0.24 us -> 6.66 us
    all_gather x1 -> x0, waiting for transfers between devices: 138 us -> none  [local(): lax.all_gather(down_weight.astype(jnp.bfloat16), FS, axis=1, tiled=True)]
    all_gather x1, waiting for transfers between devices: 106 us -> 176 us  [local(): upward_full = lax.all_gather(upward_bf, FS, axis=0, tiled=True)]
    all_to_all x2, blocking collectives: 55.6 us -> 37.6 us  [sum_at_owner(): lax.all_to_all(tiles, axis, split_axis=0, concat_axis=0, tiled=True)]
    all_to_all x0 -> x1, starting transfers between devices: none -> 6.46 us  [local(): lax.all_to_all(jnp.stack([down_weight.astype(jnp.bfloat16)] * lax.axis_si...]
  transfers between devices with their start and end apart: 6 -> 6, of which waited for: 6 -> 5; matrix products, arithmetic and copies ran while one was open for 7% -> 9% of each run, Pallas kernels for 0% -> 0%
where the time goes in v1:
time: 559 us; the launch traced here: 558 us
  waiting for transfers between devices  414 us (74%)
  blocking collectives  56.6 us (10%)
  matrix products  43.3 us (8%)
  between operations  13.4 us (2%)
  other arithmetic  12.5 us (2%)
  local copies, waits for them, and re-layouts  11.9 us (2%)
  starting transfers between devices  6.66 us (1%)
    all_gather x1, waiting for transfers between devices, local(): upward_full = lax.all_gather(upward_bf, FS, axis=0, tiled=True)  176 us
    all_gather x1, waiting for transfers between devices, in_one_piece(): lax.all_gather(both, axis, axis=dim, tiled=True)  150 us
    all_gather x1, waiting for transfers between devices, stacked_from(): tiles = lax.all_gather(tiles, axes[k])  41.1 us
    all_to_all x2, blocking collectives, sum_at_owner(): lax.all_to_all(tiles, axis, split_axis=0, concat_axis=0, tiled=True)  37.6 us
    all_gather x1, waiting for transfers between devices, local(): grouped_first = lax.all_gather(first, 'tp', axis=0, tiled=True)  33 us
    all_gather x2, blocking collectives, stacked_from(): tiles = lax.all_gather(tiles, axes[k])  19 us
    dot_general x1, matrix products, local(): jnp.dot(selected, mixout_full, preferred_element_type=jnp.float32)  13.9 us
    all_gather x1, waiting for transfers between devices, local(): grouped = lax.all_gather(tokens, 'tp', axis=0, tiled=True)  13.4 us
  transfers between devices with their start and end apart: 6, of which 5 were waited for; matrix products, arithmetic and copies ran while one was open for 9% of the time, Pallas kernels for 0%

profile of v1, /device:TPU:1, one launch (start us, length us, event | category | flops | bytes accessed | tf_op | source)
XLA Modules:
  0.0 558.5 jit_solution(9543314783399947747)
XLA Ops:
  6.5 0.0 all-gather.17.cloned.1.call-start
  6.6 1.0 convert_element_type.53
  7.6 5.6 %all-gather = bf16[1536,64]{0,1:T(8,128)(2,1)S(1)} all-gather(bf16[768,64]{0,1:T(8,128)(2,1)S(1)} %convert_element_type.53), channel_id=2, replica_groups=mesh['rep'=2,'fs_0'=2,'fs_1'=4,'fs_2'=4,'tp'=2] {'fs_0'}, dimensions={0}, use_global_device_ids=true | all-gather | bytes 294912 | tf_op jit(solution)/shard_map/all_gather | solution.py:32
  13.2 0.0 copy-start.3
  13.3 13.4 %all-gather.1 = bf16[8,768,64]{1,2,0:T(8,128)(2,1)} all-gather(bf16[2,768,64]{1,2,0:T(8,128)(2,1)S(1)} %bitcast.40), channel_id=3, replica_groups=mesh['rep'=2,'fs_0'=2,'fs_1'=4,'fs_2'=4,'tp'=2] {'fs_1'}, dimensions={0}, use_global_device_ids=true | all-gather | bytes 983040 | tf_op jit(solution)/shard_map/all_gather | solution.py:32
  26.6 0.0 all-gather.17.cloned.1.call-update
  26.6 0.0 all-gather.11.cloned.1.call-start
  26.7 0.7 all-gather.11.cloned.1.call-update
  27.4 0.0 all-gather.9.cloned.1.call-start
  27.4 0.0 copy-done.4
  27.5 0.0 copy-done.5
  27.5 0.0 copy-done.6
  27.5 0.7 pad_maximum_fusion
  28.3 0.0 all-gather.9.cloned.1.call-update
  28.3 0.0 all-gather.15.cloned.1.call-start
  28.4 0.7 convert_element_type.58
  29.1 0.0 all-gather.15.cloned.1.call-update
  29.2 0.0 copy-done.9
  29.2 41.1 %all-gather.17.cloned.1.call-done = bf16[16,2,768,64]{2,3,1,0:T(8,128)(2,1)} async-done(((bf16[4,2,768,64]{2,3,1,0:T(8,128)(2,1)}), bf16[16,2,768,64]{2,3,1,0:T(8,128)(2,1)}) %all-gather.17.cloned.1.call-update) | async-done | bytes 3145744 | tf_op jit(solution)/shard_map/all_gather | solution.py:32
  70.4 3.9 copy.16
  74.3 13.4 %all-gather.11.cloned.1.call-done = bf16[768,2048]{1,0:T(8,128)(2,1)} async-done(((bf16[384,2048]{1,0:T(8,128)(2,1)}), bf16[768,2048]{1,0:T(8,128)(2,1)}) %all-gather.11.cloned.1.call-update) | async-done | bytes 3145744 | tf_op jit(solution)/shard_map/all_gather | solution.py:82
  87.7 149.6 %all-gather.9.cloned.1.call-done = bf16[2048,2304]{1,0:T(8,128)(2,1)} async-done(((bf16[64,2304]{1,0:T(8,128)(2,1)}), bf16[2048,2304]{1,0:T(8,128)(2,1)}) %all-gather.9.cloned.1.call-update) | async-done | bytes 9437200 | tf_op jit(solution)/shard_map/all_gather | solution.py:20
  237.2 5.6 %fusion = f32[768,768]{1,0:T(8,128)S(1)} fusion(bf16[768,2048]{1,0:T(8,128)(2,1)} %all-gather.11.cloned.1.call-done, bf16[2048,2304]{1,0:T(8,128)(2,1)} %all-gather.9.cloned.1.call-done), kind=kOutput, calls=%fused_computation.5 | convolution fusion | flops 2415919104 | bytes 8650752 | tf_op jit(solution)/shard_map/dot_general | solution.py:89
  242.9 0.0 copy-done.10
  242.9 4.6 multiply_bitcast_fusion
  247.5 2.9 fusion.21
  250.4 13.9 %convolution_convert_fusion.1 = bf16[768,2048]{1,0:T(8,128)(2,1)} fusion(bf16[768,2048]{0,1:T(8,128)(2,1)} %bitcast.35, f32[767,768]{0,1:T(8,128)} %get-tuple-element.9, f32[768,768]{0,1:T(8,128)S(1)} %multiply_bitcast_fusion, f32[767,768]{0,1:T(8,128)} %get-tuple-element.8, bf16[768,2048]{1,0:T(8,128)(2,1)} %all-gather.11.cloned.1.call-done, ...), kind=kOutput, calls=%fused_computation.4 | convolution fusion | flops 4838719488 | bytes 19671552 | tf_op jit(solution)/shard_map/dot_general | solution.py:94
  264.3 31.4 %all_to_all.15 = bf16[2,384,2048]{2,1,0:T(8,128)(2,1)} all-to-all(bf16[2,384,2048]{2,1,0:T(8,128)(2,1)} %bitcast.36), channel_id=1, replica_groups=mesh['rep'=2,'fs_0'=2,'fs_1'=4,'fs_2'=4,'tp'=2] {'tp'}, dimensions={0} | all-to-all | bytes 6291456 | tf_op jit(solution)/shard_map/all_to_all | solution.py:50
  295.7 4.4 stack.2
  300.1 6.5 %all-to-all-start.1 = ((bf16[32,2048,64]{1,2,0:T(8,128)(2,1)}), bf16[32,2048,64]{1,2,0:T(8,128)(2,1)}, u32[]{:S(2)}, u32[]{:S(2)}) async-start(bf16[32,2048,64]{1,2,0:T(8,128)(2,1)} %stack.2), calls=%async_computation.1 | async-start | bytes 16777216 | tf_op jit(solution)/shard_map/all_to_all | solution.py:108
  306.6 0.0 copy-start.1
  306.6 0.0 all-gather.13.cloned.1.call-start
  306.6 3.1 convert_reduce_fusion.1
  309.7 0.5 fusion.11
  310.2 0.7 multiply_reduce_fusion.1
  310.9 1.8 multiply_convert_fusion.2
  312.8 0.0 all-gather.13.cloned.1.call-update
  312.8 176.2 %all-gather.15.cloned.1.call-done = bf16[2048,2048]{1,0:T(8,128)(2,1)} async-done(((bf16[64,2048]{1,0:T(8,128)(2,1)}), bf16[2048,2048]{1,0:T(8,128)(2,1)}) %all-gather.15.cloned.1.call-update) | async-done | bytes 8388624 | tf_op jit(solution)/shard_map/all_gather | solution.py:103
  489.0 33.0 %all-gather.13.cloned.1.call-done = bf16[768,2048]{1,0:T(8,128)(2,1)} async-done(((bf16[384,2048]{1,0:T(8,128)(2,1)}), bf16[768,2048]{1,0:T(8,128)(2,1)}) %all-gather.13.cloned.1.call-update) | async-done | bytes 3145744 | tf_op jit(solution)/shard_map/all_gather | solution.py:101
  522.1 10.0 %multiply_convert_fusion = bf16[768,2048]{1,0:T(8,128)(2,1)S(1)} fusion(bf16[768,2048]{1,0:T(8,128)(2,1)} %all-gather.13.cloned.1.call-done, bf16[2048,2048]{1,0:T(8,128)(2,1)} %all-gather.15.cloned.1.call-done), kind=kOutput, calls=%fused_computation.1 | convolution fusion | flops 6447169536 | bytes 14680064 | tf_op jit(solution)/shard_map/dot_general | solution.py:104
  532.1 0.0 all-to-all-done.1
  532.1 9.1 %convolution_convert_fusion = bf16[768,2048]{1,0:T(8,128)(2,1)S(1)} fusion(bf16[768,2048]{1,0:T(8,128)(2,1)S(1)} %multiply_convert_fusion, bf16[2048,2048]{0,1:T(8,128)(2,1)} %bitcast.10), kind=kOutput, calls=%fused_computation.3 | convolution fusion | flops 6444023808 | bytes 14680064 | tf_op jit(solution)/shard_map/dot_general | solution.py:113
  541.3 6.2 %all_to_all.16 = bf16[2,384,2048]{2,1,0:T(8,128)(2,1)S(1)} all-to-all(bf16[2,384,2048]{2,1,0:T(8,128)(2,1)S(1)} %bitcast.37), channel_id=1, replica_groups=mesh['rep'=2,'fs_0'=2,'fs_1'=4,'fs_2'=4,'tp'=2] {'tp'}, dimensions={0} | all-to-all | bytes 6291456 | tf_op jit(solution)/shard_map/all_to_all | solution.py:50
  547.5 0.7 convert_reduce_fusion
  548.2 0.7 copy-done
  548.9 0.5 fusion.12
  549.4 0.7 multiply_reduce_fusion
  550.1 1.8 multiply_convert_fusion.1
  (25 shorter events, 0.2 us)
Async XLA Ops:
  6.5 20.9 %copy-start.4 = (f32[64,768]{1,0:T(8,128)S(1)}, f32[64,768]{1,0:T(8,128)}, u32[]{:S(2)}) copy-start(f32[64,768]{1,0:T(8,128)} %param.11) | copy-start | bytes 589828
  6.5 20.9 %copy-start.5 = (f32[64,768]{1,0:T(8,128)S(1)}, f32[64,768]{1,0:T(8,128)}, u32[]{:S(2)}) copy-start(f32[64,768]{1,0:T(8,128)} %param.12) | copy-start | bytes 589828
  6.5 21.0 %copy-start.6 = (f32[64,768]{1,0:T(8,128)S(1)}, f32[64,768]{1,0:T(8,128)}, u32[]{:S(2)}) copy-start(f32[64,768]{1,0:T(8,128)} %param.13) | copy-start | bytes 589828
  6.5 21.8 %copy-start.2 = (f32[64,2048]{1,0:T(8,128)S(1)}, f32[64,2048]{1,0:T(8,128)}, u32[]{:S(2)}) copy-start(f32[64,2048]{1,0:T(8,128)} %param.17) | copy-start | bytes 1572868
  6.5 63.8 %all-gather.17.cloned.1.call-start = ((), (), s32[]{:S(2)}) async-start(), calls=%async_computation.7 | async-start | bytes 3932160 | tf_op jit(solution)/shard_map/all_gather | solution.py:32
  13.2 15.9 %copy-start.3 = (f32[2048,64]{0,1:T(8,128)S(1)}, f32[2048,64]{0,1:T(8,128)}, u32[]{:S(2)}) copy-start(f32[2048,64]{0,1:T(8,128)} %param.18) | copy-start | bytes 1572868
  26.6 2.6 copy-start.9
  26.6 61.0 %all-gather.11.cloned.1.call-start = ((), (), s32[]{:S(2)}) async-start(), calls=%async_computation.4 | async-start | bytes 4718592 | tf_op jit(solution)/shard_map/all_gather | solution.py:82
  27.4 209.8 %all-gather.9.cloned.1.call-start = ((), (), s32[]{:S(2)}) async-start(), calls=%async_computation.3 | async-start | bytes 9732096 | tf_op jit(solution)/shard_map/all_gather | solution.py:20
  28.3 460.7 %all-gather.15.cloned.1.call-start = ((), (), s32[]{:S(2)}) async-start(), calls=%async_computation.6 | async-start | bytes 8650752 | tf_op jit(solution)/shard_map/all_gather | solution.py:103
  237.2 5.7 %copy-start.10 = (bf16[768,2048]{1,0:T(8,128)(2,1)S(1)}, bf16[768,2048]{1,0:T(8,128)(2,1)}, u32[]{:S(2)}) copy-start(bf16[768,2048]{1,0:T(8,128)(2,1)} %all-gather.11.cloned.1.call-done) | copy-start | bytes 9437188
  300.1 232.0 %all-to-all-start.1 = ((bf16[32,2048,64]{1,2,0:T(8,128)(2,1)}), bf16[32,2048,64]{1,2,0:T(8,128)(2,1)}, u32[]{:S(2)}, u32[]{:S(2)}) async-start(bf16[32,2048,64]{1,2,0:T(8,128)(2,1)} %stack.2), calls=%async_computation.1 | async-start | bytes 16777216 | tf_op jit(solution)/shard_map/all_to_all | solution.py:108
  306.6 3.1 copy-start.1
  306.6 215.5 %all-gather.13.cloned.1.call-start = ((), (), s32[]{:S(2)}) async-start(), calls=%async_computation.5 | async-start | bytes 4718592 | tf_op jit(solution)/shard_map/all_gather | solution.py:101
  310.2 0.7 copy-start.7
  547.5 1.4 copy-start
  549.4 0.7 copy-start.8
Sparse Core Ops, SparseCore 0:
  26.8 43.5 all-gather.16
  72.0 15.6 all-gather.10
  89.3 147.8 all-gather.8
  238.7 250.2 all-gather.14
  490.5 31.4 all-gather.12
